TPU v7x, 256 devices: a whole 4x4x8 slice. The times are simulated.
256 devices in a mesh: fs: 16 (over y, x), tp: 16 (over z, core).
Axes of the slice: x: 4, y: 4, z: 8, core: 2. Of those that a mesh axis runs over, the one named last changes fastest.
Arguments:
- tokens: bfloat16 [16384, 2048], P(('fs', 'tp')), may hold values from -6 to 6
- gate_weight: bfloat16 [2048, 5632], P('fs', 'tp'), may hold values from -0.125 to 0.125
- up_weight: bfloat16 [2048, 5632], P('fs', 'tp'), may hold values from -0.125 to 0.125
- down_weight: bfloat16 [5632, 2048], P('tp', 'fs'), may hold values from -0.078125 to 0.078125
- grad_out: bfloat16 [16384, 2048], P(('fs', 'tp')), may hold values from -24 to 24
Outputs:
- grad_input: bfloat16 [16384, 2048], P(('fs', 'tp'))
- grad_gate: float32 [2048, 5632], P('fs', 'tp')
- grad_up: float32 [2048, 5632], P('fs', 'tp')
- grad_down: float32 [5632, 2048], P('tp', 'fs')
All inputs are finite; a program needn't handle non-finite values.
Results may differ from a plain program's by a relative error of at most 0.0049.
Values may be sent and summed in bfloat16 or wider, within the bound.
A program may use at most 128 MiB of HBM per device.

v0:
```python
import jax
import jax.numpy as jnp
from jax import lax
from jax.sharding import PartitionSpec as P


def sent_together(arrays, axis, dim, along):
    widths = [a.shape[along] for a in arrays]
    both = jnp.concatenate(arrays, axis=along)
    whole = lax.all_gather(both, axis, axis=dim, tiled=True)
    return tuple(jnp.split(whole, [sum(widths[:k]) for k in range(1, len(widths))], axis=along))


def in_order(pieces, dim):
    dims = list(pieces.shape[1:])
    dims[dim] *= pieces.shape[0]
    return jnp.moveaxis(pieces, 0, dim).reshape(dims)


def copy_for_each(x, axis):
    length = lax.axis_size(axis)
    return lax.all_to_all(jnp.broadcast_to(x[None], (length, *x.shape)), axis, 0, 0, tiled=True)


def gather_directly(x, axis, dim):
    return in_order(copy_for_each(x, axis), dim)


def over_rows(left, right):
    return lax.dot_general(
        left, right, (((0,), (0,)), ((), ())), preferred_element_type=jnp.float32
    )


def over_cols(left, right):
    return lax.dot_general(
        left, right, (((1,), (1,)), ((), ())), preferred_element_type=jnp.float32
    )


def body(tokens, gate_weight, up_weight, down_weight, grad_out):
    tok_all, cot_all = sent_together((tokens, grad_out), "tp", 0, 1)
    gate_full, up_full = sent_together((gate_weight, up_weight), "fs", 0, 1)
    down_full = gather_directly(down_weight, "fs", 1)
    gate_pre = jnp.dot(tok_all, gate_full, preferred_element_type=jnp.float32)
    up_pre = jnp.dot(tok_all, up_full, preferred_element_type=jnp.float32)
    sig_gate = jax.nn.sigmoid(gate_pre)
    active = gate_pre * sig_gate
    hidden = (active * up_pre).astype(jnp.bfloat16)
    d_hidden = over_cols(cot_all, down_full)
    d_gate = (d_hidden * up_pre * sig_gate * (1.0 + gate_pre * (1.0 - sig_gate))).astype(
        jnp.bfloat16
    )
    d_up = (d_hidden * active).astype(jnp.bfloat16)
    grad_input = lax.psum_scatter(
        over_cols(d_gate, gate_full) + over_cols(d_up, up_full),
        "tp",
        scatter_dimension=0,
        tiled=True,
    ).astype(jnp.bfloat16)
    width = gate_full.shape[1]
    summed = lax.psum_scatter(
        jnp.concatenate(
            [over_rows(tok_all, d_gate), over_rows(tok_all, d_up), over_rows(cot_all, hidden)],
            axis=1,
        ),
        "fs",
        scatter_dimension=0,
        tiled=True,
    )
    grad_gate = summed[:, :width]
    grad_up = summed[:, width : 2 * width]
    grad_down = summed[:, 2 * width :].T
    return (grad_input, grad_gate, grad_up, grad_down)


def solution(mesh):
    in_specs = (
        P(("fs", "tp"), None),
        P("fs", "tp"),
        P("fs", "tp"),
        P("tp", "fs"),
        P(("fs", "tp"), None),
    )
    out_specs = (P(("fs", "tp"), None), P("fs", "tp"), P("fs", "tp"), P("tp", "fs"))
    return jax.shard_map(body, mesh=mesh, in_specs=in_specs, out_specs=out_specs, check_vma=False)
```

profile of v0, /device:TPU:1, one launch (start us, length us, event | category | flops | bytes accessed | tf_op | source)
XLA Modules:
  0.0 328.1 jit_solution(6695033487975725311)
XLA Ops:
  7.2 0.0 all-gather.5.cloned.1.call-start
  7.2 1.6 pad_maximum_fusion.2
  8.8 0.0 all-gather.5.cloned.1.call-update
  8.9 0.0 all-gather.3.cloned.1.call-start
  8.9 1.9 pad_maximum_fusion.1
  10.8 0.0 all-gather.3.cloned.1.call-update
  10.8 2.2 broadcast_in_dim.2
  13.0 7.6 %all-to-all-start = ((bf16[16,352,128]{2,1,0:T(8,128)(2,1)}), bf16[16,352,128]{2,1,0:T(8,128)(2,1)}, u32[]{:S(2)}, u32[]{:S(2)}) async-start(bf16[16,352,128]{2,1,0:T(8,128)(2,1)} %broadcast_in_dim.2), calls=%async_computation | async-start | bytes 2883584 | tf_op jit(solution)/shard_map/all_to_all | solution.py:22
  20.6 0.0 reduce-scatter.3.cloned.1.call-start
  20.7 56.5 %all-gather.5.cloned.1.call-done = bf16[2048,704]{0,1:T(8,128)(2,1)} async-done(((bf16[128,704]{0,1:T(8,128)(2,1)}), bf16[2048,704]{0,1:T(8,128)(2,1)}) %all-gather.5.cloned.1.call-update) | async-done | bytes 2883600 | tf_op jit(solution)/shard_map/all_gather | solution.py:10
  77.2 0.0 copy-start
  77.2 58.9 %all-gather.3.cloned.1.call-done = bf16[1024,4096]{1,0:T(8,128)(2,1)} async-done(((bf16[64,4096]{1,0:T(8,128)(2,1)}), bf16[1024,4096]{1,0:T(8,128)(2,1)}) %all-gather.3.cloned.1.call-update) | async-done | bytes 8388624 | tf_op jit(solution)/shard_map/all_gather | solution.py:10
  136.1 0.0 copy-start.5
  136.1 5.6 %fusion.8 = f32[1024,352]{0,1:T(8,128)} fusion(bf16[1024,4096]{1,0:T(8,128)(2,1)} %all-gather.3.cloned.1.call-done, bf16[2048,704]{0,1:T(8,128)(2,1)} %all-gather.5.cloned.1.call-done), kind=kOutput, calls=%fused_computation.10 | convolution fusion | flops 1476395008 | bytes 7077888 | tf_op jit(solution)/shard_map/dot_general | solution.py:45
  141.7 0.0 copy-done
  141.7 0.0 copy-done.5
  141.7 2.8 fusion.10
  144.5 0.0 all-to-all-done
  144.5 5.5 %multiply_convert_fusion.1 = (bf16[1024,352]{0,1:T(8,128)(2,1)S(1)}, bf16[1024,352]{0,1:T(8,128)(2,1)S(1)}) fusion(f32[1024,352]{0,1:T(8,128)} %fusion.8, f32[1024,352]{0,1:T(8,128)} %fusion.10, bf16[1024,4096]{1,0:T(8,128)(2,1)} %all-gather.3.cloned.1.call-done, bf16[16,352,128]{2,1,0:T(8,128)(2,1)} %all-to-all-done), kind=kOutput, calls=%fused_computation.17 | convolution fusion | flops 1481080832 | bytes 9961472 | tf_op jit(solution)/shard_map/dot_general | solution.py:36
  150.0 0.0 copy-start.3
  150.0 0.0 copy-start.1
  150.0 2.4 fusion.15
  152.4 0.0 copy-done.3
  152.4 0.0 copy-done.1
  152.4 5.9 %convolution_add_fusion = f32[1024,2048]{1,0:T(8,128)} fusion(f32[1024,2048]{1,0:T(8,128)S(1)} %fusion.15, bf16[1024,352]{0,1:T(8,128)(2,1)S(1)} %get-tuple-element.4, bf16[2048,704]{0,1:T(8,128)(2,1)S(1)} %copy-done), kind=kOutput, calls=%fused_computation.1 | convolution fusion | flops 1478492160 | bytes 18939904 | tf_op jit(solution)/shard_map/dot_general | solution.py:36
  158.3 0.0 copy-start.2
  158.3 0.0 reduce-scatter.3.cloned.1.call-update
  158.3 0.0 copy-start.4
  158.3 0.2 reduce-scatter.5.cloned.1.call-start
  158.5 0.8 copy-done.2
  159.4 3.8 %fusion.6 = f32[2048,352]{0,1:T(8,128)S(1)} fusion(bf16[1024,352]{0,1:T(8,128)(2,1)S(1)} %copy-done.2, bf16[1024,4096]{1,0:T(8,128)(2,1)} %all-gather.3.cloned.1.call-done), kind=kOutput, calls=%fused_computation.8 | convolution fusion | flops 1476395008 | bytes 7798784 | tf_op jit(solution)/shard_map/dot_general | solution.py:30
  163.2 0.0 copy-done.4
  163.2 0.0 copy-start.6
  163.3 0.0 copy-start.7
  163.3 4.0 %fusion.4 = f32[2048,352]{0,1:T(8,128)S(1)} fusion(bf16[1024,352]{0,1:T(8,128)(2,1)S(1)} %copy-done.4, bf16[1024,4096]{1,0:T(8,128)(2,1)} %all-gather.3.cloned.1.call-done), kind=kOutput, calls=%fused_computation.6 | convolution fusion | flops 1476395008 | bytes 7798784 | tf_op jit(solution)/shard_map/dot_general | solution.py:30
  167.3 0.0 copy-done.6
  167.3 0.0 copy-done.7
  167.3 4.3 %fusion = f32[2048,352]{0,1:T(8,128)S(1)} fusion(bf16[1024,4096]{1,0:T(8,128)(2,1)} %all-gather.3.cloned.1.call-done, f32[1024,352]{0,1:T(8,128)S(1)} %copy-done.7, f32[1024,352]{0,1:T(8,128)S(1)} %copy-done.6), kind=kOutput, calls=%fused_computation.2 | convolution fusion | flops 1478557696 | bytes 9961472 | tf_op jit(solution)/shard_map/dot_general | solution.py:30
  171.6 4.1 %pad_maximum_fusion = f32[2048,1056]{0,1:T(8,128)} fusion(f32[2048,352]{0,1:T(8,128)S(1)} %fusion, f32[2048,352]{0,1:T(8,128)S(1)} %fusion.6, f32[2048,352]{0,1:T(8,128)S(1)} %fusion.4), kind=kLoop, calls=%fused_computation | loop fusion | flops 4325376 | bytes 17301504 | tf_op jit(solution)/shard_map/concatenate | solution.py:63
  175.7 0.0 reduce-scatter.5.cloned.1.call-update
  175.7 48.8 %reduce-scatter.3.cloned.1.call-done = f32[64,2048]{1,0:T(8,128)} async-done(((f32[1024,2048]{1,0:T(8,128)}), f32[64,2048]{1,0:T(8,128)}) %reduce-scatter.3.cloned.1.call-update) | async-done | bytes 524304 | tf_op jit(solution)/shard_map/reduce_scatter | solution.py:55
  224.6 1.8 convert_element_type.14
  226.3 93.3 %reduce-scatter.5.cloned.1.call-done = f32[128,1056]{0,1:T(8,128)} async-done(((f32[2048,1056]{0,1:T(8,128)}), f32[128,1056]{0,1:T(8,128)}) %reduce-scatter.5.cloned.1.call-update) | async-done | bytes 540688 | tf_op jit(solution)/shard_map/reduce_scatter | solution.py:62
  319.7 1.9 slice_bitcast_fusion
Async XLA Ops:
  7.2 70.0 %all-gather.5.cloned.1.call-start = ((), (), s32[]{:S(2)}) async-start(), calls=%async_computation.4 | async-start | bytes 3063808 | tf_op jit(solution)/shard_map/all_gather | solution.py:10
  8.9 127.2 %all-gather.3.cloned.1.call-start = ((), (), s32[]{:S(2)}) async-start(), calls=%async_computation.3 | async-start | bytes 8912896 | tf_op jit(solution)/shard_map/all_gather | solution.py:10
  13.0 131.5 %all-to-all-start = ((bf16[16,352,128]{2,1,0:T(8,128)(2,1)}), bf16[16,352,128]{2,1,0:T(8,128)(2,1)}, u32[]{:S(2)}, u32[]{:S(2)}) async-start(bf16[16,352,128]{2,1,0:T(8,128)(2,1)} %broadcast_in_dim.2), calls=%async_computation | async-start | bytes 2883584 | tf_op jit(solution)/shard_map/all_to_all | solution.py:22
  20.6 203.9 %reduce-scatter.3.cloned.1.call-start = ((), (), s32[]{:S(2)}) async-start(), calls=%async_computation.5 | async-start | bytes 8912896 | tf_op jit(solution)/shard_map/reduce_scatter | solution.py:55
  77.2 64.5 %copy-start = (bf16[2048,704]{0,1:T(8,128)(2,1)S(1)}, bf16[2048,704]{0,1:T(8,128)(2,1)}, u32[]{:S(2)}) copy-start(bf16[2048,704]{0,1:T(8,128)(2,1)} %all-gather.5.cloned.1.call-done) | copy-start | bytes 8650756
  136.1 5.6 %copy-start.5 = (bf16[1024,4096]{1,0:T(8,128)(2,1)S(1)}, bf16[1024,4096]{1,0:T(8,128)(2,1)}, u32[]{:S(2)}) copy-start(bf16[1024,4096]{1,0:T(8,128)(2,1)} %all-gather.3.cloned.1.call-done) | copy-start | bytes 25165828
  150.0 2.4 copy-start.3
  150.0 2.4 copy-start.1
  158.3 1.1 copy-start.2
  158.3 4.9 %copy-start.4 = (bf16[1024,352]{0,1:T(8,128)(2,1)S(1)}, bf16[1024,352]{0,1:T(8,128)(2,1)}, u32[]{:S(2)}) copy-start(bf16[1024,352]{0,1:T(8,128)(2,1)} %copy-done.3) | copy-start | bytes 2162692
  158.3 161.4 %reduce-scatter.5.cloned.1.call-start = ((), (), s32[]{:S(2)}) async-start(), calls=%async_computation.6 | async-start | bytes 9191424 | tf_op jit(solution)/shard_map/reduce_scatter | solution.py:62
  163.2 4.0 %copy-start.6 = (f32[1024,352]{0,1:T(8,128)S(1)}, f32[1024,352]{0,1:T(8,128)}, u32[]{:S(2)}) copy-start(f32[1024,352]{0,1:T(8,128)} %fusion.8) | copy-start | bytes 4325380
  163.3 4.0 %copy-start.7 = (f32[1024,352]{0,1:T(8,128)S(1)}, f32[1024,352]{0,1:T(8,128)}, u32[]{:S(2)}) copy-start(f32[1024,352]{0,1:T(8,128)} %fusion.10) | copy-start | bytes 4325380
Sparse Core Ops, SparseCore 0:
  11.0 66.1 all-gather.4
  79.0 57.0 all-gather.2
  158.4 66.1 reduce-scatter.2
  228.2 91.4 reduce-scatter.4
where the time goes:
time: 329 us; the launch traced here: 328 us
  waiting for transfers between devices  258 us (78%)
  matrix products  34.3 us (10%)
  between operations  13.9 us (4%)
  other arithmetic  9.42 us (3%)
  starting transfers between devices  7.96 us (2%)
  local copies, waits for them, and re-layouts  4.94 us (2%)
    all_gather x2, waiting for transfers between devices, sent_together(): whole = lax.all_gather(both, axis, axis=dim, tiled=True)  115 us
    reduce_scatter x1, waiting for transfers between devices, body(): lax.psum_scatter(jnp.concatenate([over_rows(tok_all, d_gate), over_rows(t...  93.3 us
    reduce_scatter x1, waiting for transfers between devices, body(): lax.psum_scatter(over_cols(d_gate, gate_full) + over_cols(d_up, up_full),...  48.8 us
    dot_general x3, matrix products, over_cols(): lax.dot_general(left, right, (((1,), (1,)), ((), ())), preferred_element_...  13.7 us
    dot_general x3, matrix products, over_rows(): lax.dot_general(left, right, (((0,), (0,)), ((), ())), preferred_element_...  12.1 us
    all_to_all x1, starting transfers between devices, copy_for_each(): lax.all_to_all(jnp.broadcast_to(x[None], (length, *x.shape)), axis, 0, 0,...  7.62 us
  transfers between devices with their start and end apart: 5, of which 4 were waited for; matrix products, arithmetic and copies ran while one was open for 9% of the time, Pallas kernels for 0%

commit v1 on v0

v1 whole, which is shorter than its diff:
```python
import jax
import jax.numpy as jnp
from jax import lax
from jax.experimental import pallas as pl
from jax.experimental.pallas import tpu as pltpu
from jax.sharding import PartitionSpec as P

BF16 = jnp.bfloat16
F32 = jnp.float32
D, HID, ROWS = 2048, 352, 64
ALL = 3 * HID
NX, NY, NZ = 4, 4, 8
PAIR = 4 * ROWS
SUB = (((0, 272), (272, 528)), ((528, 800), (800, 1056)))
PLACE = {0: 0, -1: 1, 1: 2, -2: 3, 2: 4, -3: 5, 3: 6, 4: 7}
LINK_RATE, CORE_RATE, LATENCY = 46.6e3, 600e3, 2.0
GATHER = 0
SEGMENTS = 12


def slot(rel, other_core):
    return 2 * PLACE[rel] + other_core


class Task:
    def __init__(self, name, link, size, deps, copy, before=None):
        self.name, self.link, self.size, self.deps = name, link, size, deps
        self.copy, self.before = copy, before


def in_time_order(tasks, start=0.0):
    arrival, free, order, left = {}, {}, [], list(tasks)
    while left:
        best = None
        for task in left:
            if all(dep in arrival for dep in task.deps):
                ready = max([start] + [arrival[dep] for dep in task.deps])
                if best is None or ready < best[0] - 1e-9:
                    best = (ready, task)
        ready, task = best
        left.remove(task)
        order.append((ready, task))
        if task.link is None:
            arrival[task.name] = ready
        else:
            rate = CORE_RATE if task.link == "core" else LINK_RATE
            begin = max(ready, free.get(task.link, 0.0))
            free[task.link] = begin + task.size / rate
            arrival[task.name] = free[task.link] + LATENCY
    return order, arrival


def kernel(tok, gate_t, up_t, down, cot, grad_in, o_gate, o_up, o_down,
           w, xg, yg, mix, mix_t, gi, pair_in, gw,
           z_out, z_in, f_out, f_in, s_out, s_in,
           load_sem, send_sem, recv_sem):
    fs, tp = lax.axis_index("fs"), lax.axis_index("tp")
    y, x, z, core = fs // NX, fs % NX, tp // 2, tp % 2

    def device(link):
        if link == "core":
            return {"fs": fs, "tp": z * 2 + (1 - core)}
        step = 1 if link[1] == "+" else -1
        if link[0] == "z":
            return {"fs": fs, "tp": (z + NZ + step) % NZ * 2 + core}
        if link[0] == "x":
            return {"fs": y * NX + (x + NX + step) % NX, "tp": tp}
        return {"fs": (y + NY + step) % NY * NX + x, "tp": tp}

    def columns(dy, dx):
        owner = (y + NY + dy) % NY * NX + (x + NX + dx) % NX
        return pl.ds(pl.multiple_of(owner * 128, 128), 128)

    loads = [
        pltpu.make_async_copy(tok, xg.at[pl.ds(0, ROWS)], load_sem.at[0]),
        pltpu.make_async_copy(cot, yg.at[pl.ds(0, ROWS)], load_sem.at[1]),
        pltpu.make_async_copy(gate_t, w.at[pl.ds(0, HID), columns(0, 0)], load_sem.at[2]),
        pltpu.make_async_copy(up_t, w.at[pl.ds(HID, HID), columns(0, 0)], load_sem.at[3]),
        pltpu.make_async_copy(down, w.at[pl.ds(2 * HID, HID), columns(0, 0)], load_sem.at[4]),
    ]
    for load in loads:
        load.start()
    barrier = pltpu.get_barrier_semaphore()
    links = ("x+", "x-", "y+", "y-", "z+", "z-", "core")
    for link in links:
        pl.semaphore_signal(barrier, inc=1, device_id=device(link),
                            device_id_type=pl.DeviceIdType.MESH)
    pl.semaphore_wait(barrier, len(links))
    for load in loads:
        load.wait()

    number = {}

    def remote(name, link, src, dst):
        k = number.setdefault(name, len(number))
        return pltpu.make_async_remote_copy(
            src_ref=src, dst_ref=dst, send_sem=send_sem.at[k], recv_sem=recv_sem.at[k],
            device_id=device(link), device_id_type=pl.DeviceIdType.MESH)

    gather = []

    def add_tokens(name, link, ref, src, dst, deps):
        gather.append(Task(name, link, ROWS * D * 2, deps, lambda: remote(
            name, link, ref.at[pl.ds(ROWS * src, ROWS)], ref.at[pl.ds(ROWS * dst, ROWS)])))

    def add_weights(name, link, rows, dy, dx, deps):
        place = lambda: w.at[pl.ds(rows[0], rows[1] - rows[0]), columns(dy, dx)]
        gather.append(Task(name, link, (rows[1] - rows[0]) * 256, deps,
                           lambda: remote(name, link, place(), place())))

    both = (("x", xg), ("y", yg))
    for hop in range(1, 5):
        for sign, mark in ((1, "+"), (-1, "-")):
            for unit, ref in both:
                if hop == 4 and unit != ("x" if sign > 0 else "y"):
                    continue
                rel = -sign * hop if hop < 4 else 4
                add_tokens(("t", unit, rel), "z" + mark, ref, slot(-sign * (hop - 1), 0),
                           slot(rel, 0), [("t", unit, -sign * (hop - 1))] if hop > 1 else [])
    for rel in (0, -1, 1, -2, 2, -3, 3, 4):
        for unit, ref in both:
            add_tokens(("p", unit, rel), "core", ref, slot(rel, 0), slot(rel, 1),
                       [("t", unit, rel)] if rel else [])

    axes = (("x", "y"), ("y", "x"))

    def at(half, first, second):
        return (second, first) if half == 0 else (first, second)

    for stage in (1, 2):
        for half in (0, 1):
            whole = (SUB[half][0][0], SUB[half][1][1])
            axis = axes[half][stage - 1]
            for q in ((0,) if stage == 1 else (0, -1, 1, 2)):
                for sign, mark in ((1, "+"), (-1, "-")):
                    spot = (lambda r: at(half, r, 0)) if stage == 1 else (lambda r: at(half, q, r))
                    if stage == 1 or q == 0:
                        deps = []
                    elif q == 2:
                        deps = [("w", half, 1, 0, 2, 0), ("w", half, 1, 0, 2, 1)]
                    else:
                        deps = [("w", half, 1, 0, q)]
                    add_weights(("w", half, stage, q, -sign), axis + mark, whole, *spot(0), deps)
                for k, (sign, mark) in enumerate(((1, "+"), (-1, "-"))):
                    add_weights(("w", half, stage, q, 2, k), axis + mark, SUB[half][k],
                                *spot(-sign), [("w", half, stage, q, -sign)])

    order, arrival = in_time_order(gather, LATENCY)
    by_name = {task.name: task for task in gather}
    waited = set()

    def wait_for(name):
        if name not in waited:
            waited.add(name)
            by_name[name].copy().wait_recv()

    def run(tasks):
        for task in tasks:
            for dep in task.deps:
                wait_for(dep)
            if task.before is not None:
                task.before()
            if task.copy is not None:
                task.copy().start()

    gw[...] = jnp.zeros_like(gw)
    run([task for _, task in order])
    for task in sorted(gather, key=lambda t: arrival[t.name]):
        wait_for(task.name)

    def compute(p):
        rows = pl.ds(pl.multiple_of(p * PAIR, PAIR), PAIR)
        nt = (((1,), (1,)), ((), ()))
        pre = lax.dot_general(w[0:2 * HID, :], xg[rows, :], nt, preferred_element_type=F32)
        d_hidden = lax.dot_general(w[2 * HID:, :], yg[rows, :], nt, preferred_element_type=F32)
        gate, up = pre[:HID], pre[HID:]
        sig = jax.nn.sigmoid(gate)
        active = gate * sig
        mix[2 * HID:, :] = (active * up).astype(BF16)
        mix[0:HID, :] = (d_hidden * up * sig * (1.0 + gate * (1.0 - sig))).astype(BF16)
        mix[HID:2 * HID, :] = (d_hidden * active).astype(BF16)
        mix_t[...] = mix[0:2 * HID, :].T
        for n in range(0, D, 512):
            gi[rows, n:n + 512] = jnp.dot(mix_t[...], w[0:2 * HID, n:n + 512],
                                          preferred_element_type=F32)
        for n in range(0, D, 256):
            gw[0:2 * HID, n:n + 256] += jnp.dot(mix[0:2 * HID, :], xg[rows, n:n + 256],
                                                preferred_element_type=F32)
            gw[2 * HID:, n:n + 256] += jnp.dot(mix[2 * HID:, :], yg[rows, n:n + 256],
                                               preferred_element_type=F32)

    @pl.loop(0, 4)
    def _(p):
        compute(p)

    scatter = []
    half_cols = D // 2

    def add_sum(name, link, deps, make, out, into, size):
        def before():
            out()[...] = make().astype(BF16)
        scatter.append(Task(name, link, size, deps,
                            lambda: remote(name, link, out(), into()), before))

    for rel in (4, -3, 3, -2, 2, -1, 1, 0):
        def copy(rel=rel):
            return remote(("c", rel), "core", gi.at[pl.ds(ROWS * slot(rel, 1), ROWS)],
                          pair_in.at[PLACE[rel]])
        scatter.append(Task(("c", rel), "core", ROWS * D * 4, [], copy))

    def own_tokens(rel, c):
        cols = pl.ds(c * half_cols, half_cols)
        return gi[pl.ds(ROWS * slot(rel, 0), ROWS), cols] + pair_in[PLACE[rel], :, cols]

    for left in (4, 3, 2, 1):
        for k, mark in enumerate("+-"):
            for c in ((1 - k, k) if left < 4 else (k,)):
                rel = left if left == 4 or k == 0 else -left
                earlier = ("z", k, left + 1, c)
                fresh = left == 4 or (left == 3 and c != k)
                place = lambda buf, k=k, left=left, c=c: buf.at[k, left - 1, c]
                def make(rel=rel, c=c, k=k, left=left, fresh=fresh):
                    own = own_tokens(rel, c)
                    return own if fresh else own + z_in[k, left, c].astype(F32)
                add_sum(("z", k, left, c), "z" + mark,
                        [("c", rel)] + ([] if fresh else [earlier]), make,
                        lambda place=place: place(z_out), lambda place=place: place(z_in),
                        ROWS * half_cols * 2)

    def final_tokens(c):
        total = own_tokens(0, c) + z_in[0, 0, c].astype(F32) + z_in[1, 0, c].astype(F32)
        grad_in[:, pl.ds(c * half_cols, half_cols)] = total.astype(BF16)

    for c in (0, 1):
        scatter.append(Task(("zf", c), None, 0, [("c", 0), ("z", 0, 1, c), ("z", 1, 1, c)],
                            None, lambda c=c: final_tokens(c)))

    sum_axes = (("y", "x"), ("x", "y"))
    QS = {2: 0, 1: 1, -1: 2, 0: 3}

    def local(half, s):
        a, b = SUB[half][s]
        return pl.ds(a - SUB[half][0][0], b - a)

    def target(half, first, second):
        return columns(first, second) if half == 0 else columns(second, first)

    def own_grad(half, s, ra, q):
        a, b = SUB[half][s]
        return gw[pl.ds(a, b - a), target(half, ra, q)]

    def reduced(half, s, q):
        here = local(half, s)
        return (own_grad(half, s, 0, q) + f_in[half, 0, QS[q], 0, here].astype(F32)
                + f_in[half, 1, QS[q], 0, here].astype(F32))

    def reduced_deps(half, s, q):
        return [("f", half, q, 0, 1, s), ("f", half, q, 1, 1, s)]

    for kind in (0, 1, 2):
        for q in (2, 1, -1, 0):
            for half in (0, 1):
                for k, mark in enumerate("+-"):
                    sign = 1 - 2 * k
                    far, s = (2, k) if kind == 0 else (1, 1 - k if kind == 1 else k)
                    place = lambda buf, half=half, k=k, q=q, far=far, s=s: (
                        buf.at[half, k, QS[q], far - 1, local(half, s)])
                    def make(half=half, s=s, q=q, k=k, far=far, sign=sign, kind=kind):
                        own = own_grad(half, s, sign * far if far == 1 else 2, q)
                        if kind < 2:
                            return own
                        return own + f_in[half, k, QS[q], 1, local(half, s)].astype(F32)
                    add_sum(("f", half, q, k, far, s), sum_axes[half][0] + mark,
                            [("f", half, q, k, 2, s)] if kind == 2 else [], make,
                            lambda place=place: place(f_out), lambda place=place: place(f_in),
                            (SUB[half][s][1] - SUB[half][s][0]) * 256)
    for kind in (0, 1, 2):
        for half in (0, 1):
            for k, mark in enumerate("+-"):
                sign = 1 - 2 * k
                far, s = (2, k) if kind == 0 else (1, 1 - k if kind == 1 else k)
                q = 2 if far == 2 else sign
                place = lambda buf, half=half, k=k, far=far, s=s: (
                    buf.at[half, k, far - 1, local(half, s)])
                def make(half=half, s=s, q=q, k=k, kind=kind):
                    own = reduced(half, s, q)
                    if kind < 2:
                        return own
                    return own + s_in[half, k, 1, local(half, s)].astype(F32)
                add_sum(("s", half, k, far, s), sum_axes[half][1] + mark,
                        reduced_deps(half, s, q)
                        + ([("s", half, k, 2, s)] if kind == 2 else []), make,
                        lambda place=place: place(s_out), lambda place=place: place(s_in),
                        (SUB[half][s][1] - SUB[half][s][0]) * 256)

    def final_grad(half, s):
        here = local(half, s)
        total = (reduced(half, s, 0) + s_in[half, 0, 0, here].astype(F32)
                 + s_in[half, 1, 0, here].astype(F32))
        a, b = SUB[half][s]
        for m, out in enumerate((o_gate, o_up, o_down)):
            low, high = max(a, m * HID), min(b, (m + 1) * HID)
            if low < high:
                out[low - m * HID:high - m * HID, :] = total[low - a:high - a]

    for half in (0, 1):
        for s in (0, 1):
            scatter.append(Task(("sf", half, s), None, 0, reduced_deps(half, s, 0)
                                + [("s", half, k, 1, s) for k in (0, 1)],
                                None, lambda half=half, s=s: final_grad(half, s)))

    by_name.update({task.name: task for task in scatter})
    run([task for _, task in in_time_order(scatter)[0]])
    for task in gather + scatter:
        if task.copy is not None:
            wait_for(task.name) if task.name not in waited else None
            task.copy().wait_send()


COPIES = 160


def body(tokens, gate_weight, up_weight, down_weight, grad_out):
    grad = jax.ShapeDtypeStruct((HID, 128), F32)
    grad_in, g_gate, g_up, g_down = pl.pallas_call(
        kernel,
        out_shape=(jax.ShapeDtypeStruct((ROWS, D), BF16), grad, grad, grad),
        in_specs=[pl.BlockSpec(memory_space=pl.ANY)] * 5,
        out_specs=(pl.BlockSpec(memory_space=pltpu.VMEM),) * 4,
        scratch_shapes=[
            pltpu.VMEM((ALL, D), BF16),
            pltpu.VMEM((16 * ROWS, D), BF16),
            pltpu.VMEM((16 * ROWS, D), BF16),
            pltpu.VMEM((ALL, PAIR), BF16),
            pltpu.VMEM((PAIR, 2 * HID), BF16),
            pltpu.VMEM((16 * ROWS, D), F32),
            pltpu.VMEM((NZ, ROWS, D), F32),
            pltpu.VMEM((ALL, D), F32),
            pltpu.VMEM((2, 4, 2, ROWS, D // 2), BF16),
            pltpu.VMEM((2, 4, 2, ROWS, D // 2), BF16),
            pltpu.VMEM((2, 2, 4, 2, 528, 128), BF16),
            pltpu.VMEM((2, 2, 4, 2, 528, 128), BF16),
            pltpu.VMEM((2, 2, 2, 528, 128), BF16),
            pltpu.VMEM((2, 2, 2, 528, 128), BF16),
            pltpu.SemaphoreType.DMA((5,)),
            pltpu.SemaphoreType.DMA((COPIES,)),
            pltpu.SemaphoreType.DMA((COPIES,)),
        ],
        compiler_params=pltpu.CompilerParams(
            collective_id=0, has_side_effects=True, vmem_limit_bytes=66_000_000),
        name="layer",
    )(tokens, gate_weight.T, up_weight.T, down_weight, grad_out)
    return grad_in, g_gate.T, g_up.T, g_down


def solution(mesh):
    in_specs = (
        P(("fs", "tp"), None),
        P("fs", "tp"),
        P("fs", "tp"),
        P("tp", "fs"),
        P(("fs", "tp"), None),
    )
    out_specs = (P(("fs", "tp"), None), P("fs", "tp"), P("fs", "tp"), P("tp", "fs"))
    return jax.shard_map(body, mesh=mesh, in_specs=in_specs, out_specs=out_specs, check_vma=False)
```

time: 329 us -> 104 us (0.32)
  waiting for transfers between devices: 258 us -> 0 us
  Pallas kernels: 0 us -> 99.3 us
  matrix products: 34.3 us -> 0 us
  between operations: 13.9 us -> 0.65 us
  other arithmetic: 9.42 us -> 0 us
  starting transfers between devices: 7.96 us -> 0 us
    reduce_scatter x2 -> x0, waiting for transfers between devices: 142 us -> none  [the longest x1 93.3 us: body(): lax.psum_scatter(jnp.concatenate([over_rows(tok_all, d_gate), over_rows(t...]
    all_gather x2 -> x0, waiting for transfers between devices: 115 us -> none  [sent_together(): whole = lax.all_gather(both, axis, axis=dim, tiled=True)]
    pallas_call x0 -> x1, Pallas kernels: none -> 99.3 us  [body(): pl.pallas_call(kernel, out_shape=(jax.ShapeDtypeStruct((ROWS, D), BF16),...]
    dot_general x8 -> x0, matrix products: 34.3 us -> none  [the longest x3 13.7 us: over_cols(): lax.dot_general(left, right, (((1,), (1,)), ((), ())), preferred_element_...]
    concatenate x3 -> x0, other arithmetic: 7.65 us -> none  [the longest x1 4.12 us: body(): jnp.concatenate([over_rows(tok_all, d_gate), over_rows(tok_all, d_up), ov...]
    all_to_all x1 -> x0, starting transfers between devices: 7.62 us -> none  [copy_for_each(): lax.all_to_all(jnp.broadcast_to(x[None], (length, *x.shape)), axis, 0, 0,...]
    unnamed x16 -> x10, local copies, waits for them, and re-layouts: 0.87 us -> 4.36 us
  transfers between devices with their start and end apart: 5 -> 0, of which waited for: 4 -> 0; matrix products, arithmetic and copies ran while one was open for 9% -> 0% of each run, Pallas kernels for 0% -> 0%
where the time goes in v1:
time: 104 us
  Pallas kernels  99.3 us (95%)
  local copies, waits for them, and re-layouts  4.36 us (4%)
    pallas_call x1, Pallas kernels, body(): pl.pallas_call(kernel, out_shape=(jax.ShapeDtypeStruct((ROWS, D), BF16),...  99.3 us
    unnamed x10, local copies, waits for them, and re-layouts  4.36 us

profile of v1, /device:TPU:1, one launch (start us, length us, event | category | flops | bytes accessed | tf_op | source)
XLA Modules:
  0.0 104.3 jit_solution(8657277313240769019)
XLA Ops:
  0.6 99.3 %layer.1 = (bf16[64,2048]{1,0:T(8,128)(2,1)}, f32[352,128]{1,0:T(8,128)}, f32[352,128]{1,0:T(8,128)}, f32[352,128]{1,0:T(8,128)}) custom-call(bf16[64,2048]{1,0:T(8,128)(2,1)} %tok.1, bf16[352,128]{1,0:T(8,128)(2,1)} %bitcast.6, bf16[352,128]{1,0:T(8,128)(2,1)} %bitcast.7, bf16[352,128]{1,0:T(8,128)(2,1)} %down.1, bf16[64,2048]{1,0:T(8,128)(2,1)} %cot.1), custom_call_target="tpu_custom_call" | custom-call | tf_op jit(solution)/shard_map/layer/pallas_call | solution.py:325
  99.9 0.0 copy-start.2
  99.9 1.7 %copy.13 = bf16[64,2048]{1,0:T(8,128)(2,1)} copy(bf16[64,2048]{1,0:T(8,128)(2,1)} %get-tuple-element.16) | data formatting | bytes 524288
  101.6 0.0 copy-done.2
  101.7 0.0 copy-start.1
  101.7 0.7 copy.14
  102.3 0.3 copy-done.1
  102.6 0.0 copy-start
  102.6 0.7 copy.15
  103.3 0.3 copy-done
  103.6 0.7 copy.16
Async XLA Ops:
  99.9 1.7 %copy-start.2 = (f32[352,128]{1,0:T(8,128)S(1)}, f32[352,128]{1,0:T(8,128)}, u32[]{:S(2)}) copy-start(f32[352,128]{1,0:T(8,128)} %get-tuple-element.9) | copy-start | bytes 540676
  101.7 1.0 copy-start.1
  102.6 1.0 copy-start

commit v2 on v1

--- a/solution.py
+++ b/solution.py
@@ -14,8 +14,6 @@
 SUB = (((0, 272), (272, 528)), ((528, 800), (800, 1056)))
 PLACE = {0: 0, -1: 1, 1: 2, -2: 3, 2: 4, -3: 5, 3: 6, 4: 7}
 LINK_RATE, CORE_RATE, LATENCY = 46.6e3, 600e3, 2.0
-GATHER = 0
-SEGMENTS = 12
 
 
 def slot(rel, other_core):
@@ -149,27 +147,33 @@
     by_name = {task.name: task for task in gather}
     waited = set()
 
-    def wait_for(name):
-        if name not in waited:
-            waited.add(name)
-            by_name[name].copy().wait_recv()
-
-    def run(tasks):
+    def steps_of(tasks, needs=()):
+        steps = []
         for task in tasks:
-            for dep in task.deps:
-                wait_for(dep)
+            for name in task.deps:
+                if name not in waited:
+                    waited.add(name)
+                    steps.append((name, None))
+            steps.append((None, task))
+        for name in needs:
+            if name not in waited:
+                waited.add(name)
+                steps.append((name, None))
+        return steps
+
+    def run(steps):
+        for name, task in steps:
+            if task is None:
+                by_name[name].copy().wait_recv()
+                continue
             if task.before is not None:
                 task.before()
             if task.copy is not None:
                 task.copy().start()
 
     gw[...] = jnp.zeros_like(gw)
-    run([task for _, task in order])
-    for task in sorted(gather, key=lambda t: arrival[t.name]):
-        wait_for(task.name)
-
-    def compute(p):
-        rows = pl.ds(pl.multiple_of(p * PAIR, PAIR), PAIR)
+
+    def forward(rows):
         nt = (((1,), (1,)), ((), ()))
         pre = lax.dot_general(w[0:2 * HID, :], xg[rows, :], nt, preferred_element_type=F32)
         d_hidden = lax.dot_general(w[2 * HID:, :], yg[rows, :], nt, preferred_element_type=F32)
@@ -179,19 +183,44 @@
         mix[2 * HID:, :] = (active * up).astype(BF16)
         mix[0:HID, :] = (d_hidden * up * sig * (1.0 + gate * (1.0 - sig))).astype(BF16)
         mix[HID:2 * HID, :] = (d_hidden * active).astype(BF16)
+
+    def input_grad(rows):
         mix_t[...] = mix[0:2 * HID, :].T
         for n in range(0, D, 512):
             gi[rows, n:n + 512] = jnp.dot(mix_t[...], w[0:2 * HID, n:n + 512],
                                           preferred_element_type=F32)
+
+    def weight_grad(rows):
         for n in range(0, D, 256):
             gw[0:2 * HID, n:n + 256] += jnp.dot(mix[0:2 * HID, :], xg[rows, n:n + 256],
                                                 preferred_element_type=F32)
             gw[2 * HID:, n:n + 256] += jnp.dot(mix[2 * HID:, :], yg[rows, n:n + 256],
                                                preferred_element_type=F32)
 
+    parts = ((forward, 2.0), (input_grad, 1.2), (weight_grad, 1.2))
+    due, clock = {}, 0.0
+    for p in range(4):
+        rels = [rel for rel in PLACE if PLACE[rel] // 2 == p]
+        needs = [t.name for t in gather if (t.name[0] == "w" and p == 0)
+                 or (t.name[0] != "w" and t.name[2] in rels)]
+        clock = max([clock] + [arrival[name] for name in needs])
+        for j, (_, cost) in enumerate(parts):
+            tasks = [t for ready, t in order if ready <= clock]
+            order = order[len(tasks):]
+            due[p, j] = steps_of(tasks, sorted(needs, key=arrival.get) if j == 0 else ())
+            clock += cost
+    assert not order
+
     @pl.loop(0, 4)
     def _(p):
-        compute(p)
+        rows = pl.ds(pl.multiple_of(p * PAIR, PAIR), PAIR)
+        for j, (part, _) in enumerate(parts):
+            for k in range(4):
+                if due[k, j]:
+                    @pl.when(p == k)
+                    def _():
+                        run(due[k, j])
+            part(rows)
 
     scatter = []
     half_cols = D // 2
@@ -310,22 +339,32 @@
                                 None, lambda half=half, s=s: final_grad(half, s)))
 
     by_name.update({task.name: task for task in scatter})
-    run([task for _, task in in_time_order(scatter)[0]])
+    run(steps_of([task for _, task in in_time_order(scatter)[0]]))
     for task in gather + scatter:
         if task.copy is not None:
-            wait_for(task.name) if task.name not in waited else None
             task.copy().wait_send()
 
 
 COPIES = 160
+
+
+def write_out(*refs):
+    sources, results, sem = refs[:4], refs[4:8], refs[8]
+    copies = [pltpu.make_async_copy(a, b, sem.at[k])
+              for k, (a, b) in enumerate(zip(sources, results))]
+    for copy in copies:
+        copy.start()
+    for copy in copies:
+        copy.wait()
 
 
 def body(tokens, gate_weight, up_weight, down_weight, grad_out):
     grad = jax.ShapeDtypeStruct((HID, 128), F32)
-    grad_in, g_gate, g_up, g_down = pl.pallas_call(
+    shapes = (jax.ShapeDtypeStruct((ROWS, D), BF16), grad, grad, grad)
+    sums = pl.pallas_call(
         kernel,
-        out_shape=(jax.ShapeDtypeStruct((ROWS, D), BF16), grad, grad, grad),
-        in_specs=[pl.BlockSpec(memory_space=pl.ANY)] * 5,
+        out_shape=shapes,
+        in_specs=[pl.BlockSpec(memory_space=pltpu.HBM)] * 5,
         out_specs=(pl.BlockSpec(memory_space=pltpu.VMEM),) * 4,
         scratch_shapes=[
             pltpu.VMEM((ALL, D), BF16),
@@ -347,9 +386,19 @@
             pltpu.SemaphoreType.DMA((COPIES,)),
         ],
         compiler_params=pltpu.CompilerParams(
-            collective_id=0, has_side_effects=True, vmem_limit_bytes=66_000_000),
+            collective_id=0, has_side_effects=True, vmem_limit_bytes=54_000_000),
         name="layer",
-    )(tokens, gate_weight.T, up_weight.T, down_weight, grad_out)
+    )(*(pltpu.with_memory_space_constraint(v, pltpu.HBM)
+        for v in (tokens, gate_weight.T, up_weight.T, down_weight, grad_out)))
+    grad_in, g_gate, g_up, g_down = pl.pallas_call(
+        write_out,
+        out_shape=shapes,
+        in_specs=[pl.BlockSpec(memory_space=pltpu.VMEM)] * 4,
+        out_specs=(pl.BlockSpec(memory_space=pltpu.HBM),) * 4,
+        scratch_shapes=[pltpu.SemaphoreType.DMA((4,))],
+        compiler_params=pltpu.CompilerParams(vmem_limit_bytes=4_000_000),
+        name="write_out",
+    )(*sums)
     return grad_in, g_gate.T, g_up.T, g_down
 
 

time: 104 us -> 88 us (0.85)
  Pallas kernels: 99.3 us -> 87.2 us
  local copies, waits for them, and re-layouts: 4.36 us -> 0 us
    pallas_call x1 -> x2, Pallas kernels: 99.3 us -> 87.2 us  [the longest x1 86.3 us: body(): pl.pallas_call(kernel, out_shape=shapes, in_specs=[pl.BlockSpec(memory_sp...]
    unnamed x10 -> x0, local copies, waits for them, and re-layouts: 4.36 us -> none
where the time goes in v2:
time: 88 us; the launch traced here: 87.9 us
  Pallas kernels  87.2 us (99%)
    pallas_call x1, Pallas kernels, body(): pl.pallas_call(kernel, out_shape=shapes, in_specs=[pl.BlockSpec(memory_sp...  86.3 us

profile of v2, /device:TPU:1, one launch (start us, length us, event | category | flops | bytes accessed | tf_op | source)
XLA Modules:
  0.0 87.9 jit_solution(12614336120482945443)
XLA Ops:
  0.6 86.3 %layer.1 = (bf16[64,2048]{1,0:T(8,128)(2,1)S(1)}, f32[352,128]{1,0:T(8,128)S(1)}, f32[352,128]{1,0:T(8,128)S(1)}, f32[352,128]{1,0:T(8,128)S(1)}) custom-call(bf16[64,2048]{1,0:T(8,128)(2,1)} %tok.1, bf16[352,128]{1,0:T(8,128)(2,1)} %bitcast.4, bf16[352,128]{1,0:T(8,128)(2,1)} %bitcast.5, bf16[352,128]{1,0:T(8,128)(2,1)} %down.1, bf16[64,2048]{1,0:T(8,128)(2,1)} %cot.1), custom_call_target="tpu_custom_call" | custom-call | tf_op jit(solution)/shard_map/layer/pallas_call | solution.py:364
  87.0 0.9 %write_out.1 = (bf16[64,2048]{1,0:T(8,128)(2,1)}, f32[352,128]{1,0:T(8,128)}, f32[352,128]{1,0:T(8,128)}, f32[352,128]{1,0:T(8,128)}) custom-call(bf16[64,2048]{1,0:T(8,128)(2,1)S(1)} %get-tuple-element.12.refs_0_, f32[352,128]{1,0:T(8,128)S(1)} %get-tuple-element.13.refs_1_, f32[352,128]{1,0:T(8,128)S(1)} %get-tuple-element.14.refs_2_, ...), custom_call_target="tpu_custom_call" | custom-call | tf_op jit(solution)/shard_map/write_out/pallas_call | solution.py:393
